TPU v7x, 32 devices: a whole 2x2x4 slice. The times are simulated.
32 devices in a mesh: ep: 8 (over z, x), tp: 4 (over y, core).
Axes of the slice: x: 2, y: 2, z: 4, core: 2. Of those that a mesh axis runs over, the one named last changes fastest.
Arguments:
- conv_input: bfloat16 [4096, 2048], P(('ep', 'tp')), may hold values from -6 to 6
- conv_kernel: float32 [31, 2048], replicated, may hold values from -1 to 1
- conv_gain: float32 [2048], replicated, may hold values from 0.1 to 1.9
- out_weight: bfloat16 [2048, 2048], P(None, 'tp'), may hold values from -0.125 to 0.125
- moe_input: bfloat16 [4096, 2048], P(('ep', 'tp')), may hold values from -6 to 6
- moe_gain: float32 [2048], replicated, may hold values from 0.1 to 1.9
- expert_gate: bfloat16 [8, 2048, 2048], P('ep', None, 'tp'), may hold values from -0.125 to 0.125
- expert_up: bfloat16 [8, 2048, 2048], P('ep', None, 'tp'), may hold values from -0.125 to 0.125
- expert_down: bfloat16 [8, 2048, 2048], P('ep', 'tp'), may hold values from -0.125 to 0.125
- shared_gate: bfloat16 [2048, 128], replicated, may hold values from -0.125 to 0.125
- shared_up: bfloat16 [2048, 128], replicated, may hold values from -0.125 to 0.125
- shared_down: bfloat16 [128, 2048], replicated, may hold values from -0.5 to 0.5
- expert_index: int32 [4096, 2], P('ep'), may hold values from 0 to 7, all different within a row; in each aligned block of 128 rows (0 to 127, 128 to 255, ...) at most 48 rows name the same one
- routing_weight: float32 [4096, 2], P(('ep', 'tp')), may hold values from 0.25 to 1.5
Outputs:
- conv_out: bfloat16 [4096, 2048], P('ep', 'tp')
- moe_out: bfloat16 [4096, 2048], P(('ep', 'tp'))
Inputs may be any that keep to these rules, and one draw needn't show every extreme that they name: `expert_index`: each row names 2 different experts. In each aligned block of 128 rows no expert is named by more than 48 of the rows, and in some blocks one expert is named by exactly 48 rows.
All inputs are finite; a program needn't handle non-finite values.
Results may differ from a plain program's by a relative error of at most 0.009.
Values may be sent and summed in bfloat16 or wider, within the bound.
A program may use at most 128 MiB of HBM per device.

v0:
```python
import functools

import jax
import jax.numpy as jnp
from jax import lax
from jax.experimental import pallas as pl
from jax.experimental.pallas import tpu as pltpu
from jax.sharding import PartitionSpec as P

NORM_EPS = 1e-05


def passed_along(block, axis, distance):
    devices = range(lax.axis_size(axis))
    route = [(i - distance, i) for i in devices if i - distance in devices]
    return lax.ppermute(block, axis, route)


def layer_scale(row_data, gain_vec):
    values = row_data.astype(jnp.float32)
    center = values - jnp.mean(values, axis=-1, keepdims=True)
    spread = jnp.mean(center * center, axis=-1, keepdims=True)
    return center * lax.rsqrt(spread + NORM_EPS) * gain_vec


def depthwise(padded, kernel, length):
    running = jnp.zeros((length, padded.shape[1]), jnp.float32)
    for offset in range(kernel.shape[0]):
        running = running + padded[offset : offset + length].astype(jnp.float32) * kernel[offset]
    return running


def slot_table(block_index, experts, slot_count):
    onehot = (
        block_index[:, :, None] == jnp.arange(experts, dtype=jnp.int32)[None, None, :]
    ).astype(jnp.int32)
    before = jnp.cumsum(onehot, axis=1) - onehot
    position = jnp.sum(before * onehot, axis=2)
    return block_index * slot_count + position


def fill_slots(row_data, entry_slot, top_count, total_slots):
    block_count = entry_slot.shape[0]
    entries = entry_slot.shape[1]
    block_ids = jnp.arange(block_count, dtype=jnp.int32)[:, None]
    source = jnp.arange(entries, dtype=jnp.int32)[None, :] // top_count
    slot_row = (
        jnp.zeros((block_count, total_slots), jnp.int32).at[block_ids, entry_slot].set(source)
    )
    filled = jnp.zeros((block_count, total_slots), jnp.int32).at[block_ids, entry_slot].set(1)
    picked = row_data[block_ids, slot_row]
    return jnp.where(filled[:, :, None] > 0, picked, jnp.zeros((), row_data.dtype))


def gated(row_data, gate_weight, up_weight):
    gate_proj = jnp.dot(row_data, gate_weight, preferred_element_type=jnp.float32)
    up_proj = jnp.dot(row_data, up_weight, preferred_element_type=jnp.float32)
    return (jax.nn.silu(gate_proj) * up_proj).astype(jnp.bfloat16)


def on_device(
    conv_input,
    conv_kernel,
    conv_gain,
    out_weight,
    moe_input,
    moe_gain,
    expert_gate,
    expert_up,
    expert_down,
    shared_gate,
    shared_up,
    shared_down,
    expert_index,
    routing_weight,
):
    reach = conv_kernel.shape[0] - 1
    length = conv_input.shape[0]
    halo_rows = passed_along(conv_input[length - reach :], ("ep", "tp"), 1)
    padded = jnp.concatenate([halo_rows, conv_input], axis=0)
    mixed_rows = depthwise(padded, conv_kernel, length)
    normed = jax.nn.silu(layer_scale(mixed_rows, conv_gain)).astype(jnp.bfloat16)
    conv_out = jnp.dot(
        lax.all_gather(normed, "tp", axis=0, tiled=True),
        out_weight,
        preferred_element_type=jnp.float32,
    ).astype(jnp.bfloat16)
    tp_parts = lax.axis_size("tp")
    tp_index = lax.axis_index("tp")
    ep_ranks = lax.axis_size("ep")
    tok_count = moe_input.shape[0]
    top_count = routing_weight.shape[1]
    model_width = moe_input.shape[1]
    experts = ep_ranks * expert_gate.shape[0]
    slot_count = 3 * tok_count * top_count // (2 * experts)
    total_slots = experts * slot_count
    normal = layer_scale(moe_input, moe_gain).astype(jnp.bfloat16)
    group_slots = slot_table(
        expert_index.reshape(tp_parts, tok_count * top_count), experts, slot_count
    )
    own_slots = lax.dynamic_index_in_dim(group_slots, tp_index, 0, keepdims=True)
    gate_local = expert_gate[0]
    up_local = expert_up[0]
    down_local = expert_down[0]
    own_rows = fill_slots(normal[None], own_slots, top_count, total_slots)
    own_rows = own_rows.reshape(ep_ranks, slot_count, model_width)
    arrived = lax.all_to_all(own_rows, "ep", split_axis=0, concat_axis=0, tiled=True)
    hidden = gated(
        lax.all_gather(
            arrived.reshape(ep_ranks * slot_count, model_width), "tp", axis=0, tiled=True
        ),
        gate_local,
        up_local,
    )
    summed = lax.psum_scatter(
        jnp.dot(hidden, down_local, preferred_element_type=jnp.float32).astype(jnp.bfloat16),
        "tp",
        scatter_dimension=0,
        tiled=True,
    )
    returned = lax.all_to_all(
        summed.reshape(ep_ranks, slot_count, model_width),
        "ep",
        split_axis=0,
        concat_axis=0,
        tiled=True,
    )
    picked = returned.reshape(total_slots, model_width)[own_slots[0]]
    picked = picked.reshape(tok_count, top_count, model_width).astype(jnp.float32)
    routed = jnp.sum(picked * routing_weight[:, :, None], axis=1)
    shared_hidden = gated(normal, shared_gate, shared_up)
    shared_part = jnp.dot(shared_hidden, shared_down, preferred_element_type=jnp.float32)
    moe_out = (shared_part + routed).astype(jnp.bfloat16)
    return (conv_out, moe_out)


LANES = 128
ROW_TILE = 16
COLS = 512
MESH = pl.DeviceIdType.MESH


def fused_kernel(
    n,
    slots,
    reach,
    conv_in,
    taps,
    conv_gain,
    out_w_hbm,
    moe_in,
    moe_gain,
    gate_hbm,
    up_hbm,
    down_hbm,
    sh_gate,
    sh_up,
    sh_down,
    index_ref,
    weight_ref,
    conv_out,
    moe_out,
    own,
    gath,
    part,
    from_core,
    pair_sum,
    from_y,
    result,
    returned,
    normal,
    halo,
    pad,
    mixed,
    conv_all,
    gate_w,
    up_w,
    down_w,
    out_w,
    local_sem,
    chunk_send,
    chunk_recv,
    conv_send,
    conv_recv,
):
    tokens, width = moe_in.shape
    e = lax.axis_index("ep")
    t = lax.axis_index("tp")
    core = lax.rem(t, 2)
    row = t // 2
    core_peer = row * 2 + (1 - core)
    y_peer = (1 - row) * 2 + core
    diagonal = (1 - row) * 2 + (1 - core)
    place = e * 4 + t
    after = lax.rem(place + 1, n * 4)
    ahead = lax.rem(place + n * 4 - 1, n * 4)
    halo_rows = halo.shape[0]
    half = n // 2

    fetches = [
        pltpu.make_async_copy(src, dst, local_sem.at[i])
        for i, (src, dst) in enumerate(
            ((gate_hbm.at[0], gate_w), (up_hbm.at[0], up_w), (down_hbm.at[0], down_w), (out_w_hbm, out_w))
        )
    ]
    for fetch in fetches:
        fetch.start()

    barrier = pltpu.get_barrier_semaphore()
    greeted = [(lax.rem(e + k, n), t) for k in range(1, n)]
    greeted += [(e, core_peer), (e, y_peer)]
    greeted += [(after // 4, lax.rem(after, 4)), (ahead // 4, lax.rem(ahead, 4))]
    for device in greeted:
        pl.semaphore_signal(barrier, inc=1, device_id=device, device_id_type=MESH)
    pl.semaphore_wait(barrier, len(greeted))

    def remote(src, dst, kind, k, device):
        return pltpu.make_async_remote_copy(
            src_ref=src,
            dst_ref=dst,
            send_sem=chunk_send.at[kind, k],
            recv_sem=chunk_recv.at[kind, k],
            device_id=device,
            device_id_type=MESH,
        )

    def conv_copy(src, dst, kind, device):
        return pltpu.make_async_remote_copy(
            src_ref=src,
            dst_ref=dst,
            send_sem=conv_send.at[kind],
            recv_sem=conv_recv.at[kind],
            device_id=device,
            device_id_type=MESH,
        )

    def hop(k):
        odd = lax.rem(k, 2)
        return odd * (half + k // 2) + (1 - odd) * lax.rem(half - k // 2, half)

    def dispatch_copy(k):
        return remote(own.at[k], gath.at[k, t], 0, k, (lax.rem(e + hop(k), n), t))

    def share_core(k, q):
        return remote(gath.at[k, q], gath.at[k, q], 1, k, (e, core_peer))

    def share_y(k, q):
        return remote(gath.at[k, q], gath.at[k, q], 2, k, (e, y_peer))

    def forward_core(k, q):
        return remote(gath.at[k, q], gath.at[k, q], 3, k, (e, core_peer))

    def reduce_core(k, q, which):
        return remote(part.at[k, q], from_core.at[which, k], 4 + which, k, (e, core_peer))

    def reduce_y(k):
        return remote(pair_sum.at[k], from_y.at[k], 6, k, (e, y_peer))

    def return_copy(k):
        return remote(result.at[k], returned.at[k], 7, k, (lax.rem(e - hop(k) + n, n), t))

    halo_copy = conv_copy(
        conv_in.at[pl.ds(tokens - halo_rows, halo_rows)],
        halo,
        0,
        (after // 4, lax.rem(after, 4)),
    )
    halo_copy.start()

    def normal_rows(i, carry):
        rows = pl.ds(pl.multiple_of(i * ROW_TILE, ROW_TILE), ROW_TILE)
        normal[rows, :] = layer_scale(moe_in[rows, :], moe_gain[...]).astype(jnp.bfloat16)
        return carry

    lax.fori_loop(0, tokens // ROW_TILE, normal_rows, 0)

    def column(row_data):
        return jnp.broadcast_to(row_data, (LANES, tokens)).T[:, 0:1]

    chosen = index_ref[:, pl.ds(pl.multiple_of(t * tokens, tokens), tokens)]
    relative = chosen - e
    relative = jnp.where(relative < 0, relative + n, relative)
    order = jnp.where(relative >= half, 2 * (relative - half) + 1, 2 * (half - relative))
    order = jnp.where(order == n, 0, order).astype(jnp.float32)
    first, second = column(order[0:1, :]), column(order[1:2, :])
    lane = lax.broadcasted_iota(jnp.int32, (tokens, LANES), 1).astype(jnp.float32)
    hot_first = (lane == first).astype(jnp.float32)
    hot_second = (lane == second).astype(jnp.float32)
    earlier = (
        lax.broadcasted_iota(jnp.int32, (tokens, tokens), 0)
        > lax.broadcasted_iota(jnp.int32, (tokens, tokens), 1)
    ).astype(jnp.float32).astype(jnp.bfloat16)
    before = jnp.dot(
        earlier, (hot_first + hot_second).astype(jnp.bfloat16), preferred_element_type=jnp.float32
    )
    slot_first = first * slots + jnp.sum(before * hot_first, axis=1, keepdims=True)
    slot_second = second * slots + jnp.sum(
        before * hot_second, axis=1, keepdims=True
    )
    row_first = jnp.broadcast_to(slot_first, (tokens, LANES)).T[0:1, :]
    row_second = jnp.broadcast_to(slot_second, (tokens, LANES)).T[0:1, :]
    slot_row = lax.broadcasted_iota(jnp.int32, (n * slots, tokens), 0).astype(jnp.float32)
    spread = (
        jnp.where(slot_row == row_first, 1.0, 0.0) + jnp.where(slot_row == row_second, 1.0, 0.0)
    ).astype(jnp.bfloat16)
    for c in range(0, width, COLS):
        rows = jnp.dot(spread, normal[:, c : c + COLS], preferred_element_type=jnp.float32)
        rows = rows.astype(jnp.bfloat16).reshape(n, slots, COLS)
        own[:, :, c : c + COLS] = rows
        gath[0, t, :, c : c + COLS] = rows[0]

    for k in range(1, n):
        dispatch_copy(k).start()

    def relay(k):
        share_y(k, t).start()
        share_core(k, t).start()

    def forward(k):
        share_y(k, y_peer).wait_recv()
        forward_core(k, y_peer).start()

    relay(0)

    conv_copy(halo, halo, 0, (e, core_peer)).wait_recv()
    inside = jnp.where(place == 0, 0.0, 1.0)
    pad[0:halo_rows, :] = halo[...].astype(jnp.float32) * inside
    pad[halo_rows:, :] = conv_in[...].astype(jnp.float32)

    def strip(c, carry):
        cols = pl.ds(pl.multiple_of(c * LANES, LANES), LANES)
        total = jnp.zeros((tokens, LANES), jnp.float32)
        for k in range(reach + 1):
            start = halo_rows - reach + k
            total = total + pad[pl.ds(start, tokens), cols] * taps[pl.ds(k, 1), cols]
        mixed[:, cols] = total
        return carry

    lax.fori_loop(0, width // LANES, strip, 0)

    def conv_rows(i, carry):
        rows = pl.ds(pl.multiple_of(i * ROW_TILE, ROW_TILE), ROW_TILE)
        conv_all[t, rows, :] = jax.nn.silu(layer_scale(mixed[rows, :], conv_gain[...])).astype(
            jnp.bfloat16
        )
        return carry

    lax.fori_loop(0, tokens // ROW_TILE, conv_rows, 0)
    conv_y = conv_copy(conv_all.at[t], conv_all.at[t], 1, (e, y_peer))
    conv_core = conv_copy(conv_all.at[t], conv_all.at[t], 2, (e, core_peer))
    conv_pass = conv_copy(conv_all.at[y_peer], conv_all.at[y_peer], 3, (e, core_peer))
    conv_y.start()
    conv_core.start()

    dispatch_copy(1).wait_recv()
    relay(1)
    forward(0)
    for fetch in fetches[:3]:
        fetch.wait()

    def step(i, carry):
        @pl.when(i + 2 < n)
        def _():
            k = i + 2
            dispatch_copy(k).wait_recv()
            relay(k)

        @pl.when(i + 1 < n)
        def _():
            forward(i + 1)

        @pl.when(i == 2)
        def _():
            conv_copy(conv_all.at[y_peer], conv_all.at[y_peer], 1, (e, y_peer)).wait_recv()
            conv_pass.start()

        @pl.when(i < n)
        def _():
            share_core(i, core_peer).wait_recv()
            forward_core(i, diagonal).wait_recv()
            rows = gath[i].reshape(4 * slots, width)
            hidden = gated(rows, gate_w[...], up_w[...])
            for c in range(0, width, COLS):
                piece = jnp.dot(hidden, down_w[:, c : c + COLS], preferred_element_type=jnp.float32)
                part[i, :, :, c : c + COLS] = piece.astype(jnp.bfloat16).reshape(4, slots, COLS)
            reduce_core(i, diagonal, 1).start()
            reduce_core(i, core_peer, 0).start()

        @pl.when((i >= 1) & (i <= n))
        def _():
            k = i - 1
            reduce_core(k, core_peer, 1).wait_recv()
            pair_sum[k] = (
                part[k, y_peer].astype(jnp.float32) + from_core[1, k].astype(jnp.float32)
            ).astype(jnp.bfloat16)
            reduce_y(k).start()

        @pl.when(i >= 2)
        def _():
            k = i - 2
            reduce_core(k, core_peer, 0).wait_recv()
            reduce_y(k).wait_recv()
            total = part[k, t].astype(jnp.float32) + from_core[0, k].astype(jnp.float32)
            total = (total + from_y[k].astype(jnp.float32)).astype(jnp.bfloat16)

            @pl.when(k > 0)
            def _():
                result[k] = total
                return_copy(k).start()

            @pl.when(k == 0)
            def _():
                returned[0] = total

        return carry

    lax.fori_loop(0, n + 2, step, 0)

    conv_copy(conv_all.at[core_peer], conv_all.at[core_peer], 2, (e, core_peer)).wait_recv()
    conv_copy(conv_all.at[diagonal], conv_all.at[diagonal], 3, (e, core_peer)).wait_recv()
    fetches[3].wait()
    for q in range(4):
        conv_out[q * tokens : (q + 1) * tokens, :] = jnp.dot(
            conv_all[q], out_w[...], preferred_element_type=jnp.float32
        ).astype(jnp.bfloat16)

    shared = gated(normal[...], sh_gate[...], sh_up[...])
    slot_lane = lax.broadcasted_iota(jnp.int32, (tokens, n * slots), 1).astype(jnp.float32)
    share = jnp.where(slot_lane == slot_first, column(weight_ref[0:1, :]), 0.0) + jnp.where(
        slot_lane == slot_second, column(weight_ref[1:2, :]), 0.0
    )
    share_high = share.astype(jnp.bfloat16)
    share_low = (share - share_high.astype(jnp.float32)).astype(jnp.bfloat16)
    for k in range(1, n):
        return_copy(k).wait_recv()
    for c in range(0, width, COLS):
        rows = returned[:, :, c : c + COLS].reshape(n * slots, COLS)
        total = jnp.dot(shared, sh_down[:, c : c + COLS], preferred_element_type=jnp.float32)
        total = total + jnp.dot(share_high, rows, preferred_element_type=jnp.float32)
        total = total + jnp.dot(share_low, rows, preferred_element_type=jnp.float32)
        moe_out[:, c : c + COLS] = total.astype(jnp.bfloat16)

    halo_copy.wait_send()
    conv_y.wait_send()
    conv_core.wait_send()
    conv_pass.wait_send()

    def drain(k, carry):
        @pl.when(k > 0)
        def _():
            dispatch_copy(k).wait_send()
            return_copy(k).wait_send()

        share_y(k, t).wait_send()
        share_core(k, t).wait_send()
        forward_core(k, y_peer).wait_send()
        reduce_core(k, diagonal, 1).wait_send()
        reduce_core(k, core_peer, 0).wait_send()
        reduce_y(k).wait_send()
        return carry

    lax.fori_loop(0, n, drain, 0)


def fused(
    conv_input,
    conv_kernel,
    conv_gain,
    out_weight,
    moe_input,
    moe_gain,
    expert_gate,
    expert_up,
    expert_down,
    shared_gate,
    shared_up,
    shared_down,
    expert_index,
    routing_weight,
):
    n = lax.axis_size("ep")
    parts = lax.axis_size("tp")
    tokens, width = moe_input.shape
    slots = 3 * tokens * routing_weight.shape[1] // (2 * n)
    hidden = expert_gate.shape[2]
    reach = conv_kernel.shape[0] - 1
    halo_rows = -(-reach // ROW_TILE) * ROW_TILE
    out_cols = out_weight.shape[1]
    bf16 = jnp.bfloat16
    chunk = (n, slots, width)
    vmem = pl.BlockSpec(memory_space=pltpu.VMEM)
    hbm = pl.BlockSpec(memory_space=pl.ANY)
    return pl.pallas_call(
        functools.partial(fused_kernel, n, slots, reach),
        out_shape=(
            jax.ShapeDtypeStruct((parts * tokens, out_cols), bf16),
            jax.ShapeDtypeStruct((tokens, width), bf16),
        ),
        in_specs=[vmem, vmem, vmem, hbm, vmem, vmem, hbm, hbm, hbm, vmem, vmem, vmem, vmem, vmem],
        out_specs=(vmem, vmem),
        scratch_shapes=[
            pltpu.VMEM(chunk, bf16),
            pltpu.VMEM((n, parts, slots, width), bf16),
            pltpu.VMEM((n, parts, slots, width), bf16),
            pltpu.VMEM((2,) + chunk, bf16),
            pltpu.VMEM(chunk, bf16),
            pltpu.VMEM(chunk, bf16),
            pltpu.VMEM(chunk, bf16),
            pltpu.VMEM(chunk, bf16),
            pltpu.VMEM((tokens, width), bf16),
            pltpu.VMEM((halo_rows, width), bf16),
            pltpu.VMEM((halo_rows + tokens, width), jnp.float32),
            pltpu.VMEM((tokens, width), jnp.float32),
            pltpu.VMEM((parts, tokens, width), bf16),
            pltpu.VMEM((width, hidden), bf16),
            pltpu.VMEM((width, hidden), bf16),
            pltpu.VMEM((hidden, width), bf16),
            pltpu.VMEM((width, out_cols), bf16),
            pltpu.SemaphoreType.DMA((4,)),
            pltpu.SemaphoreType.DMA((8, n)),
            pltpu.SemaphoreType.DMA((8, n)),
            pltpu.SemaphoreType.DMA((4,)),
            pltpu.SemaphoreType.DMA((4,)),
        ],
        compiler_params=pltpu.CompilerParams(
            collective_id=0, has_side_effects=True, vmem_limit_bytes=60 * 1024 * 1024
        ),
    )(
        conv_input,
        conv_kernel,
        conv_gain.reshape(1, width),
        out_weight,
        moe_input,
        moe_gain.reshape(1, width),
        expert_gate,
        expert_up,
        expert_down,
        shared_gate,
        shared_up,
        shared_down,
        expert_index.T,
        routing_weight.T,
    )


def fits_fused(args):
    n, parts = lax.axis_size("ep"), lax.axis_size("tp")
    conv_input, conv_kernel, moe_input = args[0], args[1], args[4]
    top_count = args[13].shape[1]
    tokens, width = moe_input.shape
    slots = 3 * tokens * top_count // (2 * n)
    return (
        parts == 4
        and top_count == 2
        and args[6].shape[0] == 1
        and conv_input.shape == moe_input.shape
        and conv_kernel.shape[0] - 1 <= tokens
        and tokens % LANES == 0
        and width % COLS == 0
        and slots % ROW_TILE == 0
        and slots >= ROW_TILE
        and n <= LANES
        and n % 2 == 0
    )


def either(*args):
    return fused(*args) if fits_fused(args) else on_device(*args)


def solution(mesh):
    in_specs = (
        P(("ep", "tp"), None),
        P(),
        P(),
        P(None, "tp"),
        P(("ep", "tp"), None),
        P(),
        P("ep", None, "tp"),
        P("ep", None, "tp"),
        P("ep", "tp", None),
        P(),
        P(),
        P(),
        P("ep", None),
        P(("ep", "tp"), None),
    )
    out_specs = (P("ep", "tp"), P(("ep", "tp"), None))
    return jax.shard_map(
        either, mesh=mesh, in_specs=in_specs, out_specs=out_specs, check_vma=False
    )
```

profile of v0, /device:TPU:0, one launch (start us, length us, event | category | flops | bytes accessed | tf_op | source)
XLA Modules:
  0.0 111.9 jit_solution(17837914651313746477)
XLA Ops:
  0.6 107.5 %shard_map.149 = (bf16[512,512]{1,0:T(8,128)(2,1)}, bf16[128,2048]{1,0:T(8,128)(2,1)}) custom-call(bf16[128,2048]{1,0:T(8,128)(2,1)} %conv_in.1, f32[31,2048]{1,0:T(8,128)} %taps.1, f32[1,2048]{1,0:T(1,128)} %bitcast.4, bf16[2048,512]{1,0:T(8,128)(2,1)} %out_w_hbm.1, bf16[128,2048]{1,0:T(8,128)(2,1)} %moe_in.1, f32[1,2048]{1,0:T(1,128)} %bitcast.5, ...), custom_call_target="tpu_custom_call" | custom-call | tf_op jit(solution)/shard_map/pallas_call | solution.py:493
  108.2 1.9 %copy.18 = bf16[512,512]{1,0:T(8,128)(2,1)} copy(bf16[512,512]{1,0:T(8,128)(2,1)} %get-tuple-element.4) | data formatting | bytes 1048576
  110.1 1.9 %copy.19 = bf16[128,2048]{1,0:T(8,128)(2,1)} copy(bf16[128,2048]{1,0:T(8,128)(2,1)} %get-tuple-element.5) | data formatting | bytes 1048576
where the time goes:
time: 112 us
  Pallas kernels  108 us (96%)
  local copies, waits for them, and re-layouts  3.75 us (3%)
    pallas_call x1, Pallas kernels, fused(): pl.pallas_call(functools.partial(fused_kernel, n, slots, reach), out_shap...  108 us
    unnamed x2, local copies, waits for them, and re-layouts  3.75 us

commit v1 on v0

--- a/solution.py
+++ b/solution.py
@@ -137,6 +137,7 @@
 LANES = 128
 ROW_TILE = 16
 COLS = 512
+CONV_PARTS = 4
 MESH = pl.DeviceIdType.MESH
 
 
@@ -144,38 +145,52 @@
     n,
     slots,
     reach,
-    conv_in,
-    taps,
+    conv_hbm,
+    taps_hbm,
     conv_gain,
     out_w_hbm,
-    moe_in,
+    moe_hbm,
     moe_gain,
     gate_hbm,
     up_hbm,
     down_hbm,
-    sh_gate,
-    sh_up,
-    sh_down,
+    sh_gate_hbm,
+    sh_up_hbm,
+    sh_down_hbm,
     index_ref,
     weight_ref,
     conv_out,
     moe_out,
     own,
+    own_peer,
     gath,
     part,
     from_core,
     pair_sum,
     from_y,
     result,
+    result_peer,
     returned,
+    returned_peer,
     normal,
+    normal_peer,
+    weight_peer,
+    near_send,
+    near_recv,
+    total,
     halo,
     pad,
     mixed,
     conv_all,
+    conv_in,
+    taps,
+    moe_in,
     gate_w,
     up_w,
     down_w,
+    sh_gate,
+    sh_up,
+    sh_down,
     out_w,
     local_sem,
     chunk_send,
@@ -183,7 +198,7 @@
     conv_send,
     conv_recv,
 ):
-    tokens, width = moe_in.shape
+    tokens, width = moe_hbm.shape
     e = lax.axis_index("ep")
     t = lax.axis_index("tp")
     core = lax.rem(t, 2)
@@ -196,11 +211,27 @@
     ahead = lax.rem(place + n * 4 - 1, n * 4)
     halo_rows = halo.shape[0]
     half = n // 2
+    side = e // half
+    deep = lax.rem(e, half) // 2
+    across = lax.rem(e, 2)
+    outer = side * deep + (1 - side) * (1 - deep)
+    conv_cut = tokens // CONV_PARTS
 
     fetches = [
         pltpu.make_async_copy(src, dst, local_sem.at[i])
         for i, (src, dst) in enumerate(
-            ((gate_hbm.at[0], gate_w), (up_hbm.at[0], up_w), (down_hbm.at[0], down_w), (out_w_hbm, out_w))
+            (
+                (moe_hbm, moe_in),
+                (conv_hbm, conv_in),
+                (taps_hbm, taps),
+                (gate_hbm.at[0], gate_w),
+                (up_hbm.at[0], up_w),
+                (down_hbm.at[0], down_w),
+                (sh_gate_hbm, sh_gate),
+                (sh_up_hbm, sh_up),
+                (sh_down_hbm, sh_down),
+                (out_w_hbm, out_w),
+            )
         )
     ]
     for fetch in fetches:
@@ -212,14 +243,32 @@
     greeted += [(after // 4, lax.rem(after, 4)), (ahead // 4, lax.rem(ahead, 4))]
     for device in greeted:
         pl.semaphore_signal(barrier, inc=1, device_id=device, device_id_type=MESH)
-    pl.semaphore_wait(barrier, len(greeted))
-
-    def remote(src, dst, kind, k, device):
+
+    def flip(a, b):
+        return a + b - 2 * a * b
+
+    def near_rank(j):
+        return side * half + 2 * flip(deep, j // 2) + flip(across, lax.rem(j, 2))
+
+    def far_rank(there, j):
+        return (1 - side) * half + 2 * there + flip(across, j)
+
+    def near_item(j):
+        return 0 if j == 0 else j + 1
+
+    def is_far(k):
+        return (k == 1) | (k > half)
+
+    def far_parts(k):
+        v = (k // (half + 1)) * (k - half)
+        return v // 2, lax.rem(v, 2)
+
+    def remote(src, dst, kind, k, device, k_there=None):
         return pltpu.make_async_remote_copy(
             src_ref=src,
             dst_ref=dst,
             send_sem=chunk_send.at[kind, k],
-            recv_sem=chunk_recv.at[kind, k],
+            recv_sem=chunk_recv.at[kind, k if k_there is None else k_there],
             device_id=device,
             device_id_type=MESH,
         )
@@ -234,18 +283,27 @@
             device_id_type=MESH,
         )
 
-    def hop(k):
-        odd = lax.rem(k, 2)
-        return odd * (half + k // 2) + (1 - odd) * lax.rem(half - k // 2, half)
-
-    def dispatch_copy(k):
-        return remote(own.at[k], gath.at[k, t], 0, k, (lax.rem(e + hop(k), n), t))
+    def send_near(j):
+        k = near_item(j)
+        return remote(own.at[j], gath.at[k, t], 0, j, (near_rank(j), t), k)
+
+    def send_near_peer(j):
+        k = near_item(j)
+        return remote(own_peer.at[j], gath.at[k, y_peer], 1, k, (near_rank(j), t))
+
+    def send_far(there, j):
+        k = (1 + (half + 1) * outer) if j == 0 else (half + 1 + 2 * outer)
+        s = half + 2 * there + j
+        return remote(own.at[s], gath.at[k, t], 0, s, (far_rank(there, j), t), k)
+
+    def arrive(k):
+        return remote(own.at[k], gath.at[k, t], 0, k, (e, core_peer))
 
     def share_core(k, q):
-        return remote(gath.at[k, q], gath.at[k, q], 1, k, (e, core_peer))
+        return remote(gath.at[k, q], gath.at[k, q], 2, k, (e, core_peer))
 
     def share_y(k, q):
-        return remote(gath.at[k, q], gath.at[k, q], 2, k, (e, y_peer))
+        return remote(gath.at[k, q], gath.at[k, q], 1, k, (e, y_peer))
 
     def forward_core(k, q):
         return remote(gath.at[k, q], gath.at[k, q], 3, k, (e, core_peer))
@@ -256,16 +314,37 @@
     def reduce_y(k):
         return remote(pair_sum.at[k], from_y.at[k], 6, k, (e, y_peer))
 
-    def return_copy(k):
-        return remote(result.at[k], returned.at[k], 7, k, (lax.rem(e - hop(k) + n, n), t))
-
+    def return_near(k):
+        j = k - 1
+        return remote(result.at[k], returned.at[j], 7, k, (near_rank(j), t), j)
+
+    def return_near_peer(k):
+        j = k - 1
+        return remote(result_peer.at[k], returned_peer.at[j], 8, k, (near_rank(j), t), j)
+
+    def return_far(k):
+        m, j = far_parts(k)
+        there = m * (1 - side) + (1 - m) * side
+        s = half + 2 * deep + j
+        return remote(result.at[k], returned.at[s], 7, k, (far_rank(there, j), t), s)
+
+    normal_y = conv_copy(normal, normal_peer, 1, (e, y_peer))
+    weight_y = conv_copy(weight_ref, weight_peer, 2, (e, y_peer))
     halo_copy = conv_copy(
         conv_in.at[pl.ds(tokens - halo_rows, halo_rows)],
         halo,
         0,
         (after // 4, lax.rem(after, 4)),
     )
-    halo_copy.start()
+    conv_core = conv_copy(conv_all.at[t], conv_all.at[t], 3, (e, core_peer))
+    conv_pass = conv_copy(conv_all.at[y_peer], conv_all.at[y_peer], 4, (e, core_peer))
+    near_y = conv_copy(near_send, near_recv, 5, (e, y_peer))
+
+    def conv_y(q, p):
+        block = conv_all.at[q, pl.ds(p * conv_cut, conv_cut)]
+        return conv_copy(block, block, 6 + p, (e, y_peer))
+
+    fetches[0].wait()
 
     def normal_rows(i, carry):
         rows = pl.ds(pl.multiple_of(i * ROW_TILE, ROW_TILE), ROW_TILE)
@@ -277,63 +356,112 @@
     def column(row_data):
         return jnp.broadcast_to(row_data, (LANES, tokens)).T[:, 0:1]
 
-    chosen = index_ref[:, pl.ds(pl.multiple_of(t * tokens, tokens), tokens)]
-    relative = chosen - e
-    relative = jnp.where(relative < 0, relative + n, relative)
-    order = jnp.where(relative >= half, 2 * (relative - half) + 1, 2 * (half - relative))
-    order = jnp.where(order == n, 0, order).astype(jnp.float32)
-    first, second = column(order[0:1, :]), column(order[1:2, :])
-    lane = lax.broadcasted_iota(jnp.int32, (tokens, LANES), 1).astype(jnp.float32)
-    hot_first = (lane == first).astype(jnp.float32)
-    hot_second = (lane == second).astype(jnp.float32)
+    slot_rank = [near_rank(j) for j in range(half)]
+    slot_rank += [far_rank(s // 2, s % 2) for s in range(half)]
     earlier = (
         lax.broadcasted_iota(jnp.int32, (tokens, tokens), 0)
         > lax.broadcasted_iota(jnp.int32, (tokens, tokens), 1)
     ).astype(jnp.float32).astype(jnp.bfloat16)
-    before = jnp.dot(
-        earlier, (hot_first + hot_second).astype(jnp.bfloat16), preferred_element_type=jnp.float32
-    )
-    slot_first = first * slots + jnp.sum(before * hot_first, axis=1, keepdims=True)
-    slot_second = second * slots + jnp.sum(
-        before * hot_second, axis=1, keepdims=True
-    )
-    row_first = jnp.broadcast_to(slot_first, (tokens, LANES)).T[0:1, :]
-    row_second = jnp.broadcast_to(slot_second, (tokens, LANES)).T[0:1, :]
-    slot_row = lax.broadcasted_iota(jnp.int32, (n * slots, tokens), 0).astype(jnp.float32)
-    spread = (
-        jnp.where(slot_row == row_first, 1.0, 0.0) + jnp.where(slot_row == row_second, 1.0, 0.0)
-    ).astype(jnp.bfloat16)
+    lane = lax.broadcasted_iota(jnp.int32, (tokens, LANES), 1).astype(jnp.float32)
+
+    def slots_of(block):
+        chosen = index_ref[:, pl.ds(pl.multiple_of(block * tokens, tokens), tokens)]
+        order = jnp.zeros(chosen.shape, jnp.float32)
+        for s in range(1, n):
+            order = order + jnp.where(chosen == slot_rank[s], float(s), 0.0)
+        first, second = column(order[0:1, :]), column(order[1:2, :])
+        hot_first = (lane == first).astype(jnp.float32)
+        hot_second = (lane == second).astype(jnp.float32)
+        before = jnp.dot(
+            earlier,
+            (hot_first + hot_second).astype(jnp.bfloat16),
+            preferred_element_type=jnp.float32,
+        )
+        return (
+            first * slots + jnp.sum(before * hot_first, axis=1, keepdims=True),
+            second * slots + jnp.sum(before * hot_second, axis=1, keepdims=True),
+        )
+
+    def spread_of(pair, count):
+        row_first = jnp.broadcast_to(pair[0], (tokens, LANES)).T[0:1, :]
+        row_second = jnp.broadcast_to(pair[1], (tokens, LANES)).T[0:1, :]
+        slot_row = lax.broadcasted_iota(jnp.int32, (count * slots, tokens), 0).astype(jnp.float32)
+        return (
+            jnp.where(slot_row == row_first, 1.0, 0.0) + jnp.where(slot_row == row_second, 1.0, 0.0)
+        ).astype(jnp.bfloat16)
+
+    def share_of(pair, weights, base, count):
+        slot_lane = base * slots + lax.broadcasted_iota(
+            jnp.int32, (tokens, count * slots), 1
+        ).astype(jnp.float32)
+        share = jnp.where(slot_lane == pair[0], column(weights[0:1, :]), 0.0) + jnp.where(
+            slot_lane == pair[1], column(weights[1:2, :]), 0.0
+        )
+        high = share.astype(jnp.bfloat16)
+        return high, (share - high.astype(jnp.float32)).astype(jnp.bfloat16)
+
+    def weighed(shares, rows):
+        return jnp.dot(shares[0], rows, preferred_element_type=jnp.float32) + jnp.dot(
+            shares[1], rows, preferred_element_type=jnp.float32
+        )
+
+    pair = slots_of(t)
+    spread = spread_of(pair, n)
     for c in range(0, width, COLS):
         rows = jnp.dot(spread, normal[:, c : c + COLS], preferred_element_type=jnp.float32)
         rows = rows.astype(jnp.bfloat16).reshape(n, slots, COLS)
         own[:, :, c : c + COLS] = rows
         gath[0, t, :, c : c + COLS] = rows[0]
 
-    for k in range(1, n):
-        dispatch_copy(k).start()
-
-    def relay(k):
-        share_y(k, t).start()
-        share_core(k, t).start()
-
-    def forward(k):
-        share_y(k, y_peer).wait_recv()
-        forward_core(k, y_peer).start()
-
-    relay(0)
-
-    conv_copy(halo, halo, 0, (e, core_peer)).wait_recv()
-    inside = jnp.where(place == 0, 0.0, 1.0)
-    pad[0:halo_rows, :] = halo[...].astype(jnp.float32) * inside
+    pl.semaphore_wait(barrier, len(greeted))
+    fetches[1].wait()
+
+    @pl.when(place < n * 4 - 1)
+    def _():
+        halo_copy.start()
+
+    normal_y.start()
+    weight_y.start()
+
+    held = [(there, j) for j in range(2) for there in range(2)]
+
+    @pl.when(outer == 0)
+    def _():
+        for there, j in held:
+            send_far(there, j).start()
+
+    for j in (1, 2, 3):
+        send_near(j).start()
+
+    @pl.when(outer == 1)
+    def _():
+        send_far(*held[0]).start()
+
+    share_core(0, t).start()
+
+    fetches[2].wait()
+
+    @pl.when(place > 0)
+    def _():
+        conv_copy(halo, halo, 0, (e, core_peer)).wait_recv()
+
+    @pl.when(place > 0)
+    def _():
+        pad[0:halo_rows, :] = halo[...].astype(jnp.float32)
+
+    @pl.when(place == 0)
+    def _():
+        pad[0:halo_rows, :] = jnp.zeros((halo_rows, width), jnp.float32)
+
     pad[halo_rows:, :] = conv_in[...].astype(jnp.float32)
 
     def strip(c, carry):
         cols = pl.ds(pl.multiple_of(c * LANES, LANES), LANES)
-        total = jnp.zeros((tokens, LANES), jnp.float32)
+        running = jnp.zeros((tokens, LANES), jnp.float32)
         for k in range(reach + 1):
             start = halo_rows - reach + k
-            total = total + pad[pl.ds(start, tokens), cols] * taps[pl.ds(k, 1), cols]
-        mixed[:, cols] = total
+            running = running + pad[pl.ds(start, tokens), cols] * taps[pl.ds(k, 1), cols]
+        mixed[:, cols] = running
         return carry
 
     lax.fori_loop(0, width // LANES, strip, 0)
@@ -346,117 +474,189 @@
         return carry
 
     lax.fori_loop(0, tokens // ROW_TILE, conv_rows, 0)
-    conv_y = conv_copy(conv_all.at[t], conv_all.at[t], 1, (e, y_peer))
-    conv_core = conv_copy(conv_all.at[t], conv_all.at[t], 2, (e, core_peer))
-    conv_pass = conv_copy(conv_all.at[y_peer], conv_all.at[y_peer], 3, (e, core_peer))
-    conv_y.start()
     conv_core.start()
 
-    dispatch_copy(1).wait_recv()
+    def relay(k):
+        arrive(k).wait_recv()
+
+        @pl.when(is_far(k))
+        def _():
+            share_y(k, t).start()
+
+        share_core(k, t).start()
+
     relay(1)
-    forward(0)
-    for fetch in fetches[:3]:
+    for p in range(CONV_PARTS // 2):
+        conv_y(t, p).start()
+
+    normal_y.wait_recv()
+    pair_peer = slots_of(y_peer)
+    spread_peer = spread_of(pair_peer, half)
+    for c in range(0, width, COLS):
+        rows = jnp.dot(spread_peer, normal_peer[:, c : c + COLS], preferred_element_type=jnp.float32)
+        rows = rows.astype(jnp.bfloat16).reshape(half, slots, COLS)
+        own_peer[:, :, c : c + COLS] = rows
+        gath[0, y_peer, :, c : c + COLS] = rows[0]
+    for j in (1, 2, 3):
+        send_near_peer(j).start()
+
+    @pl.when(outer == 1)
+    def _():
+        for there, j in held[1:]:
+            send_far(there, j).start()
+
+    forward_core(0, y_peer).start()
+    relay(2)
+    for p in range(CONV_PARTS // 2, CONV_PARTS):
+        conv_y(t, p).start()
+    for fetch in fetches[3:6]:
         fetch.wait()
 
-    def step(i, carry):
-        @pl.when(i + 2 < n)
-        def _():
-            k = i + 2
-            dispatch_copy(k).wait_recv()
-            relay(k)
-
-        @pl.when(i + 1 < n)
-        def _():
-            forward(i + 1)
-
-        @pl.when(i == 2)
-        def _():
-            conv_copy(conv_all.at[y_peer], conv_all.at[y_peer], 1, (e, y_peer)).wait_recv()
-            conv_pass.start()
-
-        @pl.when(i < n)
-        def _():
-            share_core(i, core_peer).wait_recv()
-            forward_core(i, diagonal).wait_recv()
-            rows = gath[i].reshape(4 * slots, width)
-            hidden = gated(rows, gate_w[...], up_w[...])
-            for c in range(0, width, COLS):
-                piece = jnp.dot(hidden, down_w[:, c : c + COLS], preferred_element_type=jnp.float32)
-                part[i, :, :, c : c + COLS] = piece.astype(jnp.bfloat16).reshape(4, slots, COLS)
-            reduce_core(i, diagonal, 1).start()
-            reduce_core(i, core_peer, 0).start()
-
-        @pl.when((i >= 1) & (i <= n))
-        def _():
-            k = i - 1
-            reduce_core(k, core_peer, 1).wait_recv()
+    def meet_core(k):
+        reduce_core(k, core_peer, 0).wait_recv()
+        reduce_core(k, core_peer, 1).wait_recv()
+
+        @pl.when(is_far(k))
+        def _():
             pair_sum[k] = (
                 part[k, y_peer].astype(jnp.float32) + from_core[1, k].astype(jnp.float32)
             ).astype(jnp.bfloat16)
             reduce_y(k).start()
 
-        @pl.when(i >= 2)
-        def _():
-            k = i - 2
-            reduce_core(k, core_peer, 0).wait_recv()
-            reduce_y(k).wait_recv()
-            total = part[k, t].astype(jnp.float32) + from_core[0, k].astype(jnp.float32)
-            total = (total + from_y[k].astype(jnp.float32)).astype(jnp.bfloat16)
-
-            @pl.when(k > 0)
-            def _():
-                result[k] = total
-                return_copy(k).start()
-
-            @pl.when(k == 0)
-            def _():
-                returned[0] = total
+        @pl.when((k > 1) & (k <= half))
+        def _():
+            result[k] = (
+                part[k, t].astype(jnp.float32) + from_core[0, k].astype(jnp.float32)
+            ).astype(jnp.bfloat16)
+            return_near(k).start()
+            result_peer[k] = (
+                part[k, y_peer].astype(jnp.float32) + from_core[1, k].astype(jnp.float32)
+            ).astype(jnp.bfloat16)
+            return_near_peer(k).start()
+
+        @pl.when(k == 0)
+        def _():
+            returned[0] = (
+                part[0, t].astype(jnp.float32) + from_core[0, 0].astype(jnp.float32)
+            ).astype(jnp.bfloat16)
+            returned_peer[0] = (
+                part[0, y_peer].astype(jnp.float32) + from_core[1, 0].astype(jnp.float32)
+            ).astype(jnp.bfloat16)
+
+    def meet_y(k):
+        reduce_y(k).wait_recv()
+        summed = part[k, t].astype(jnp.float32) + from_core[0, k].astype(jnp.float32)
+        result[k] = (summed + from_y[k].astype(jnp.float32)).astype(jnp.bfloat16)
+        return_far(k).start()
+
+    def step(i, carry):
+        share_core(i, core_peer).wait_recv()
+        forward_core(i, diagonal).wait_recv()
+        rows = gath[i].reshape(4 * slots, width)
+        hidden = gated(rows, gate_w[...], up_w[...])
+        for c in range(0, width, COLS):
+            piece = jnp.dot(hidden, down_w[:, c : c + COLS], preferred_element_type=jnp.float32)
+            part[i, :, :, c : c + COLS] = piece.astype(jnp.bfloat16).reshape(4, slots, COLS)
+        reduce_core(i, diagonal, 1).start()
+        reduce_core(i, core_peer, 0).start()
+
+        @pl.when(i < n - 3)
+        def _():
+            relay(i + 3)
+
+        @pl.when(i + 1 < n)
+        def _():
+            share_y(i + 1, y_peer).wait_recv()
+            forward_core(i + 1, y_peer).start()
+
+        meet_core(i)
+
+        @pl.when(i == half)
+        def _():
+            for p in range(CONV_PARTS):
+                conv_y(y_peer, p).wait_recv()
+            conv_pass.start()
+            meet_y(1)
+
+        @pl.when(i == n - 1)
+        def _():
+            meet_y(n - 3)
 
         return carry
 
-    lax.fori_loop(0, n + 2, step, 0)
-
-    conv_copy(conv_all.at[core_peer], conv_all.at[core_peer], 2, (e, core_peer)).wait_recv()
-    conv_copy(conv_all.at[diagonal], conv_all.at[diagonal], 3, (e, core_peer)).wait_recv()
-    fetches[3].wait()
+    lax.fori_loop(0, n, step, 0)
+    meet_y(n - 2)
+
+    for fetch in fetches[6:]:
+        fetch.wait()
+    conv_copy(conv_all.at[core_peer], conv_all.at[core_peer], 3, (e, core_peer)).wait_recv()
+    conv_copy(conv_all.at[diagonal], conv_all.at[diagonal], 4, (e, core_peer)).wait_recv()
+
+    for j in (1, 2, 3):
+        remote(result.at[j], returned.at[j], 7, j, (e, core_peer)).wait_recv()
+        remote(result.at[j], returned_peer.at[j], 8, j, (e, core_peer)).wait_recv()
+    weight_y.wait_recv()
+    peer_share = share_of(pair_peer, weight_peer, 0, half)
+    for c in range(0, width, COLS):
+        rows = returned_peer[:, :, c : c + COLS].reshape(half * slots, COLS)
+        near_send[:, c : c + COLS] = weighed(peer_share, rows).astype(jnp.bfloat16)
+    near_y.start()
+
+    meet_y(n - 1)
+
     for q in range(4):
         conv_out[q * tokens : (q + 1) * tokens, :] = jnp.dot(
             conv_all[q], out_w[...], preferred_element_type=jnp.float32
         ).astype(jnp.bfloat16)
 
     shared = gated(normal[...], sh_gate[...], sh_up[...])
-    slot_lane = lax.broadcasted_iota(jnp.int32, (tokens, n * slots), 1).astype(jnp.float32)
-    share = jnp.where(slot_lane == slot_first, column(weight_ref[0:1, :]), 0.0) + jnp.where(
-        slot_lane == slot_second, column(weight_ref[1:2, :]), 0.0
-    )
-    share_high = share.astype(jnp.bfloat16)
-    share_low = (share - share_high.astype(jnp.float32)).astype(jnp.bfloat16)
-    for k in range(1, n):
-        return_copy(k).wait_recv()
+    near_share = share_of(pair, weight_ref, 0, half)
     for c in range(0, width, COLS):
-        rows = returned[:, :, c : c + COLS].reshape(n * slots, COLS)
-        total = jnp.dot(shared, sh_down[:, c : c + COLS], preferred_element_type=jnp.float32)
-        total = total + jnp.dot(share_high, rows, preferred_element_type=jnp.float32)
-        total = total + jnp.dot(share_low, rows, preferred_element_type=jnp.float32)
-        moe_out[:, c : c + COLS] = total.astype(jnp.bfloat16)
-
-    halo_copy.wait_send()
-    conv_y.wait_send()
-    conv_core.wait_send()
-    conv_pass.wait_send()
+        rows = returned[0:half, :, c : c + COLS].reshape(half * slots, COLS)
+        piece = jnp.dot(shared, sh_down[:, c : c + COLS], preferred_element_type=jnp.float32)
+        total[:, c : c + COLS] = piece + weighed(near_share, rows)
+
+    far_share = share_of(pair, weight_ref, half, half)
+    near_y.wait_recv()
+    for s in range(half, n):
+        remote(result.at[s], returned.at[s], 7, s, (e, core_peer)).wait_recv()
+    for c in range(0, width, COLS):
+        rows = returned[half:n, :, c : c + COLS].reshape(half * slots, COLS)
+        piece = total[:, c : c + COLS] + near_recv[:, c : c + COLS].astype(jnp.float32)
+        moe_out[:, c : c + COLS] = (piece + weighed(far_share, rows)).astype(jnp.bfloat16)
+
+    @pl.when(place < n * 4 - 1)
+    def _():
+        halo_copy.wait_send()
+
+    for copy in (normal_y, weight_y, conv_core, conv_pass, near_y):
+        copy.wait_send()
+    for p in range(CONV_PARTS):
+        conv_y(t, p).wait_send()
 
     def drain(k, carry):
         @pl.when(k > 0)
         def _():
-            dispatch_copy(k).wait_send()
-            return_copy(k).wait_send()
-
-        share_y(k, t).wait_send()
+            arrive(k).wait_send()
+
+        @pl.when(is_far(k))
+        def _():
+            share_y(k, t).wait_send()
+            reduce_y(k).wait_send()
+
+        @pl.when((k > 1) & (k <= half))
+        def _():
+            share_y(k, t).wait_send()
+            return_near_peer(k).wait_send()
+
+        @pl.when(k > 0)
+        def _():
+            remote(result.at[k], returned.at[k], 7, k, (e, core_peer)).wait_send()
+
         share_core(k, t).wait_send()
         forward_core(k, y_peer).wait_send()
         reduce_core(k, diagonal, 1).wait_send()
         reduce_core(k, core_peer, 0).wait_send()
-        reduce_y(k).wait_send()
         return carry
 
     lax.fori_loop(0, n, drain, 0)
@@ -483,23 +683,27 @@
     tokens, width = moe_input.shape
     slots = 3 * tokens * routing_weight.shape[1] // (2 * n)
     hidden = expert_gate.shape[2]
+    shared_hidden = shared_gate.shape[1]
     reach = conv_kernel.shape[0] - 1
     halo_rows = -(-reach // ROW_TILE) * ROW_TILE
     out_cols = out_weight.shape[1]
     bf16 = jnp.bfloat16
     chunk = (n, slots, width)
+    half_chunk = (n // 2, slots, width)
+    rows = (tokens, width)
     vmem = pl.BlockSpec(memory_space=pltpu.VMEM)
     hbm = pl.BlockSpec(memory_space=pl.ANY)
     return pl.pallas_call(
         functools.partial(fused_kernel, n, slots, reach),
         out_shape=(
-            jax.ShapeDtypeStruct((parts * tokens, out_cols), bf16),
-            jax.ShapeDtypeStruct((tokens, width), bf16),
+            pltpu.VMEM((parts * tokens, out_cols), bf16),
+            pltpu.VMEM(rows, bf16),
         ),
-        in_specs=[vmem, vmem, vmem, hbm, vmem, vmem, hbm, hbm, hbm, vmem, vmem, vmem, vmem, vmem],
+        in_specs=[hbm, hbm, vmem, hbm, hbm, vmem, hbm, hbm, hbm, hbm, hbm, hbm, vmem, vmem],
         out_specs=(vmem, vmem),
         scratch_shapes=[
             pltpu.VMEM(chunk, bf16),
+            pltpu.VMEM(half_chunk, bf16),
             pltpu.VMEM((n, parts, slots, width), bf16),
             pltpu.VMEM((n, parts, slots, width), bf16),
             pltpu.VMEM((2,) + chunk, bf16),
@@ -507,20 +711,33 @@
             pltpu.VMEM(chunk, bf16),
             pltpu.VMEM(chunk, bf16),
             pltpu.VMEM(chunk, bf16),
-            pltpu.VMEM((tokens, width), bf16),
+            pltpu.VMEM(chunk, bf16),
+            pltpu.VMEM(half_chunk, bf16),
+            pltpu.VMEM(rows, bf16),
+            pltpu.VMEM(rows, bf16),
+            pltpu.VMEM((2, tokens), jnp.float32),
+            pltpu.VMEM(rows, bf16),
+            pltpu.VMEM(rows, bf16),
+            pltpu.VMEM(rows, jnp.float32),
             pltpu.VMEM((halo_rows, width), bf16),
             pltpu.VMEM((halo_rows + tokens, width), jnp.float32),
-            pltpu.VMEM((tokens, width), jnp.float32),
+            pltpu.VMEM(rows, jnp.float32),
             pltpu.VMEM((parts, tokens, width), bf16),
+            pltpu.VMEM(rows, bf16),
+            pltpu.VMEM((reach + 1, width), jnp.float32),
+            pltpu.VMEM(rows, bf16),
             pltpu.VMEM((width, hidden), bf16),
             pltpu.VMEM((width, hidden), bf16),
             pltpu.VMEM((hidden, width), bf16),
+            pltpu.VMEM((width, shared_hidden), bf16),
+            pltpu.VMEM((width, shared_hidden), bf16),
+            pltpu.VMEM((shared_hidden, width), bf16),
             pltpu.VMEM((width, out_cols), bf16),
-            pltpu.SemaphoreType.DMA((4,)),
-            pltpu.SemaphoreType.DMA((8, n)),
-            pltpu.SemaphoreType.DMA((8, n)),
-            pltpu.SemaphoreType.DMA((4,)),
-            pltpu.SemaphoreType.DMA((4,)),
+            pltpu.SemaphoreType.DMA((10,)),
+            pltpu.SemaphoreType.DMA((9, n)),
+            pltpu.SemaphoreType.DMA((9, n)),
+            pltpu.SemaphoreType.DMA((6 + CONV_PARTS,)),
+            pltpu.SemaphoreType.DMA((6 + CONV_PARTS,)),
         ],
         compiler_params=pltpu.CompilerParams(
             collective_id=0, has_side_effects=True, vmem_limit_bytes=60 * 1024 * 1024
@@ -559,8 +776,7 @@
         and width % COLS == 0
         and slots % ROW_TILE == 0
         and slots >= ROW_TILE
-        and n <= LANES
-        and n % 2 == 0
+        and n == 8
     )
 
 

time: 112 us -> 95.9 us (0.86)
  Pallas kernels: 108 us -> 93.4 us
  local copies, waits for them, and re-layouts: 3.75 us -> 1.59 us
    pallas_call x1, Pallas kernels: 108 us -> 93.4 us  [fused(): pl.pallas_call(functools.partial(fused_kernel, n, slots, reach), out_shap...]
    unnamed x2, local copies, waits for them, and re-layouts: 3.75 us -> 1.59 us
where the time goes in v1:
time: 95.9 us; the launch traced here: 95.7 us
  Pallas kernels  93.4 us (97%)
  local copies, waits for them, and re-layouts  1.59 us (2%)
    pallas_call x1, Pallas kernels, fused(): pl.pallas_call(functools.partial(fused_kernel, n, slots, reach), out_shap...  93.4 us

profile of v1, /device:TPU:0, one launch (start us, length us, event | category | flops | bytes accessed | tf_op | source)
XLA Modules:
  0.0 95.7 jit_solution(17399195006111632825)
XLA Ops:
  0.6 93.4 %shard_map.149 = (bf16[512,512]{1,0:T(8,128)(2,1)S(1)}, bf16[128,2048]{1,0:T(8,128)(2,1)S(1)}) custom-call(bf16[128,2048]{1,0:T(8,128)(2,1)} %conv_hbm.1, f32[31,2048]{1,0:T(8,128)} %taps_hbm.1, f32[1,2048]{1,0:T(1,128)} %bitcast.4, bf16[2048,512]{1,0:T(8,128)(2,1)} %out_w_hbm.1, bf16[128,2048]{1,0:T(8,128)(2,1)} %moe_hbm.1, f32[1,2048]{1,0:T(1,128)} %bitcast.5, ...), custom_call_target="tpu_custom_call" | custom-call | tf_op jit(solution)/shard_map/pallas_call | solution.py:696
  94.1 0.8 copy.18
  94.9 0.8 copy.19

commit v2 on v1

--- a/solution.py
+++ b/solution.py
@@ -261,7 +261,16 @@
 
     def far_parts(k):
         v = (k // (half + 1)) * (k - half)
-        return v // 2, lax.rem(v, 2)
+        q = (v + 1) // 2
+        from_outer = (1 - outer) * (v // 2) + outer * (1 - q * (2 - q))
+        return from_outer, (1 - outer) * lax.rem(v, 2) + outer * (v // 2)
+
+    def packed(order):
+        return sum(item * n**place for place, item in enumerate(order))
+
+    item_order = (1 - outer) * packed((0, 1, 5, 2, 3, 4, 6, 7)) + outer * packed(
+        (0, 1, 2, 5, 3, 6, 4, 7)
+    )
 
     def remote(src, dst, kind, k, device, k_there=None):
         return pltpu.make_async_remote_copy(
@@ -291,8 +300,13 @@
         k = near_item(j)
         return remote(own_peer.at[j], gath.at[k, y_peer], 1, k, (near_rank(j), t))
 
-    def send_far(there, j):
-        k = (1 + (half + 1) * outer) if j == 0 else (half + 1 + 2 * outer)
+    def send_far(to_outer, j):
+        there = (1 - side) * to_outer + side * (1 - to_outer)
+        if to_outer:
+            v = (1 - outer) * (1 + j) + outer * 3 * j
+        else:
+            v = 2 * outer + j
+        k = 1 + v + 3 * ((v + 2) // 3)
         s = half + 2 * there + j
         return remote(own.at[s], gath.at[k, t], 0, s, (far_rank(there, j), t), k)
 
@@ -405,6 +419,16 @@
             shares[1], rows, preferred_element_type=jnp.float32
         )
 
+    pl.semaphore_wait(barrier, len(greeted))
+    fetches[1].wait()
+
+    @pl.when(place < n * 4 - 1)
+    def _():
+        halo_copy.start()
+
+    normal_y.start()
+    weight_y.start()
+
     pair = slots_of(t)
     spread = spread_of(pair, n)
     for c in range(0, width, COLS):
@@ -413,29 +437,17 @@
         own[:, :, c : c + COLS] = rows
         gath[0, t, :, c : c + COLS] = rows[0]
 
-    pl.semaphore_wait(barrier, len(greeted))
-    fetches[1].wait()
-
-    @pl.when(place < n * 4 - 1)
-    def _():
-        halo_copy.start()
-
-    normal_y.start()
-    weight_y.start()
-
-    held = [(there, j) for j in range(2) for there in range(2)]
-
     @pl.when(outer == 0)
     def _():
-        for there, j in held:
-            send_far(there, j).start()
-
-    for j in (1, 2, 3):
+        send_far(0, 0).start()
+        send_far(0, 1).start()
+
+    for j in (2, 3, 1):
         send_near(j).start()
 
     @pl.when(outer == 1)
     def _():
-        send_far(*held[0]).start()
+        send_far(1, 0).start()
 
     share_core(0, t).start()
 
@@ -485,9 +497,15 @@
 
         share_core(k, t).start()
 
-    relay(1)
-    for p in range(CONV_PARTS // 2):
-        conv_y(t, p).start()
+    @pl.when(outer == 0)
+    def _():
+        send_far(1, 0).start()
+        relay(1)
+
+    @pl.when(outer == 1)
+    def _():
+        for p in range(CONV_PARTS - 1):
+            conv_y(t, p).start()
 
     normal_y.wait_recv()
     pair_peer = slots_of(y_peer)
@@ -497,18 +515,26 @@
         rows = rows.astype(jnp.bfloat16).reshape(half, slots, COLS)
         own_peer[:, :, c : c + COLS] = rows
         gath[0, y_peer, :, c : c + COLS] = rows[0]
-    for j in (1, 2, 3):
+    @pl.when(outer == 1)
+    def _():
+        send_far(1, 1).start()
+
+    for j in (2, 3, 1):
         send_near_peer(j).start()
 
+    @pl.when(outer == 0)
+    def _():
+        send_far(1, 1).start()
+
     @pl.when(outer == 1)
     def _():
-        for there, j in held[1:]:
-            send_far(there, j).start()
+        send_far(0, 0).start()
+        send_far(0, 1).start()
 
     forward_core(0, y_peer).start()
     relay(2)
-    for p in range(CONV_PARTS // 2, CONV_PARTS):
-        conv_y(t, p).start()
+    relay(3)
+    relay(4)
     for fetch in fetches[3:6]:
         fetch.wait()
 
@@ -550,48 +576,81 @@
         return_far(k).start()
 
     def step(i, carry):
-        share_core(i, core_peer).wait_recv()
-        forward_core(i, diagonal).wait_recv()
-        rows = gath[i].reshape(4 * slots, width)
+        k = lax.rem(carry, n)
+        later = lax.rem(carry // n, n)
+        share_core(k, core_peer).wait_recv()
+        forward_core(k, diagonal).wait_recv()
+        rows = gath[k].reshape(4 * slots, width)
         hidden = gated(rows, gate_w[...], up_w[...])
         for c in range(0, width, COLS):
             piece = jnp.dot(hidden, down_w[:, c : c + COLS], preferred_element_type=jnp.float32)
-            part[i, :, :, c : c + COLS] = piece.astype(jnp.bfloat16).reshape(4, slots, COLS)
-        reduce_core(i, diagonal, 1).start()
-        reduce_core(i, core_peer, 0).start()
-
-        @pl.when(i < n - 3)
-        def _():
-            relay(i + 3)
+            part[k, :, :, c : c + COLS] = piece.astype(jnp.bfloat16).reshape(4, slots, COLS)
+        reduce_core(k, diagonal, 1).start()
+        reduce_core(k, core_peer, 0).start()
+
+        @pl.when((i == 0) & (outer == 1))
+        def _():
+            relay(1)
+            conv_y(t, CONV_PARTS - 1).start()
+
+        @pl.when(i == outer)
+        def _():
+            relay(5)
+
+        @pl.when((i == 0) & (outer == 0))
+        def _():
+            for p in range(CONV_PARTS // 2):
+                conv_y(t, p).start()
+
+        @pl.when((i == 2) & (outer == 1))
+        def _():
+            relay(6)
+            relay(7)
+
+        meet_first = (i == n - 1) | ((outer == 0) & (i >= 4)) | ((outer == 1) & (lax.rem(i, 2) == 0) & (i < 6))
+
+        @pl.when(meet_first)
+        def _():
+            meet_core(k)
+
+        @pl.when(i == 4)
+        def _():
+            meet_y(1)
+
+        @pl.when((i == 5) & (outer == 0))
+        def _():
+            relay(6)
+            meet_y(5)
+            relay(7)
+
+        @pl.when((i == 7) & (outer == 1))
+        def _():
+            meet_y(5)
 
         @pl.when(i + 1 < n)
         def _():
-            share_y(i + 1, y_peer).wait_recv()
-            forward_core(i + 1, y_peer).start()
-
-        meet_core(i)
-
-        @pl.when(i == half)
-        def _():
-            for p in range(CONV_PARTS):
-                conv_y(y_peer, p).wait_recv()
-            conv_pass.start()
-            meet_y(1)
-
-        @pl.when(i == n - 1)
-        def _():
-            meet_y(n - 3)
-
-        return carry
-
-    lax.fori_loop(0, n, step, 0)
-    meet_y(n - 2)
-
-    for fetch in fetches[6:]:
-        fetch.wait()
-    conv_copy(conv_all.at[core_peer], conv_all.at[core_peer], 3, (e, core_peer)).wait_recv()
-    conv_copy(conv_all.at[diagonal], conv_all.at[diagonal], 4, (e, core_peer)).wait_recv()
-
+            share_y(later, y_peer).wait_recv()
+            forward_core(later, y_peer).start()
+
+        @pl.when(jnp.logical_not(meet_first))
+        def _():
+            meet_core(k)
+
+        @pl.when((i == 2) & (outer == 0))
+        def _():
+            conv_y(t, 2).start()
+
+        return carry // n
+
+    lax.fori_loop(0, n, step, item_order)
+
+    @pl.when(outer == 0)
+    def _():
+        conv_y(t, CONV_PARTS - 1).start()
+
+    meet_y(6)
+
+    meet_y(7)
     for j in (1, 2, 3):
         remote(result.at[j], returned.at[j], 7, j, (e, core_peer)).wait_recv()
         remote(result.at[j], returned_peer.at[j], 8, j, (e, core_peer)).wait_recv()
@@ -602,7 +661,15 @@
         near_send[:, c : c + COLS] = weighed(peer_share, rows).astype(jnp.bfloat16)
     near_y.start()
 
-    meet_y(n - 1)
+
+    for p in range(CONV_PARTS):
+        conv_y(y_peer, p).wait_recv()
+    conv_pass.start()
+
+    for fetch in fetches[6:]:
+        fetch.wait()
+    conv_copy(conv_all.at[core_peer], conv_all.at[core_peer], 3, (e, core_peer)).wait_recv()
+    conv_copy(conv_all.at[diagonal], conv_all.at[diagonal], 4, (e, core_peer)).wait_recv()
 
     for q in range(4):
         conv_out[q * tokens : (q + 1) * tokens, :] = jnp.dot(

time: 95.9 us -> 91.8 us (0.957)
  Pallas kernels: 93.4 us -> 89.2 us
    pallas_call x1, Pallas kernels: 93.4 us -> 89.2 us  [fused(): pl.pallas_call(functools.partial(fused_kernel, n, slots, reach), out_shap...]
where the time goes in v2:
time: 91.8 us; the launch traced here: 91.5 us
  Pallas kernels  89.2 us (97%)
  local copies, waits for them, and re-layouts  1.59 us (2%)
    pallas_call x1, Pallas kernels, fused(): pl.pallas_call(functools.partial(fused_kernel, n, slots, reach), out_shap...  89.2 us

profile of v2, /device:TPU:0, one launch (start us, length us, event | category | flops | bytes accessed | tf_op | source)
XLA Modules:
  0.0 91.5 jit_solution(1016326262446499283)
XLA Ops:
  0.6 89.2 %shard_map.149 = (bf16[512,512]{1,0:T(8,128)(2,1)S(1)}, bf16[128,2048]{1,0:T(8,128)(2,1)S(1)}) custom-call(bf16[128,2048]{1,0:T(8,128)(2,1)} %conv_hbm.1, f32[31,2048]{1,0:T(8,128)} %taps_hbm.1, f32[1,2048]{1,0:T(1,128)} %bitcast.4, bf16[2048,512]{1,0:T(8,128)(2,1)} %out_w_hbm.1, bf16[128,2048]{1,0:T(8,128)(2,1)} %moe_hbm.1, f32[1,2048]{1,0:T(1,128)} %bitcast.5, ...), custom_call_target="tpu_custom_call" | custom-call | tf_op jit(solution)/shard_map/pallas_call | solution.py:763
  89.9 0.8 copy.18
  90.7 0.8 copy.19

commit v3 on v2

--- a/solution.py
+++ b/solution.py
@@ -358,15 +358,6 @@
         block = conv_all.at[q, pl.ds(p * conv_cut, conv_cut)]
         return conv_copy(block, block, 6 + p, (e, y_peer))
 
-    fetches[0].wait()
-
-    def normal_rows(i, carry):
-        rows = pl.ds(pl.multiple_of(i * ROW_TILE, ROW_TILE), ROW_TILE)
-        normal[rows, :] = layer_scale(moe_in[rows, :], moe_gain[...]).astype(jnp.bfloat16)
-        return carry
-
-    lax.fori_loop(0, tokens // ROW_TILE, normal_rows, 0)
-
     def column(row_data):
         return jnp.broadcast_to(row_data, (LANES, tokens)).T[:, 0:1]
 
@@ -396,10 +387,11 @@
             second * slots + jnp.sum(before * hot_second, axis=1, keepdims=True),
         )
 
-    def spread_of(pair, count):
+    def spread_of(pair, base, count):
         row_first = jnp.broadcast_to(pair[0], (tokens, LANES)).T[0:1, :]
         row_second = jnp.broadcast_to(pair[1], (tokens, LANES)).T[0:1, :]
-        slot_row = lax.broadcasted_iota(jnp.int32, (count * slots, tokens), 0).astype(jnp.float32)
+        slot_row = base * slots + lax.broadcasted_iota(jnp.int32, (count * slots, tokens), 0)
+        slot_row = slot_row.astype(jnp.float32)
         return (
             jnp.where(slot_row == row_first, 1.0, 0.0) + jnp.where(slot_row == row_second, 1.0, 0.0)
         ).astype(jnp.bfloat16)
@@ -419,6 +411,19 @@
             shares[1], rows, preferred_element_type=jnp.float32
         )
 
+    pair = slots_of(t)
+    head = (1 - outer) * half
+    spread_head = spread_of(pair, head, half)
+    spread_tail = spread_of(pair, half - head, half)
+    fetches[0].wait()
+
+    def normal_rows(i, carry):
+        rows = pl.ds(pl.multiple_of(i * ROW_TILE, ROW_TILE), ROW_TILE)
+        normal[rows, :] = layer_scale(moe_in[rows, :], moe_gain[...]).astype(jnp.bfloat16)
+        return carry
+
+    lax.fori_loop(0, tokens // ROW_TILE, normal_rows, 0, unroll=4)
+
     pl.semaphore_wait(barrier, len(greeted))
     fetches[1].wait()
 
@@ -429,26 +434,34 @@
     normal_y.start()
     weight_y.start()
 
-    pair = slots_of(t)
-    spread = spread_of(pair, n)
-    for c in range(0, width, COLS):
-        rows = jnp.dot(spread, normal[:, c : c + COLS], preferred_element_type=jnp.float32)
-        rows = rows.astype(jnp.bfloat16).reshape(n, slots, COLS)
-        own[:, :, c : c + COLS] = rows
-        gath[0, t, :, c : c + COLS] = rows[0]
-
+    def fill_own(spread, first):
+        for c in range(0, width, COLS):
+            rows = jnp.dot(spread, normal[:, c : c + COLS], preferred_element_type=jnp.float32)
+            rows = rows.astype(jnp.bfloat16).reshape(half, slots, COLS)
+            own[pl.ds(first, half), :, c : c + COLS] = rows
+
+    fill_own(spread_head, head)
     @pl.when(outer == 0)
     def _():
         send_far(0, 0).start()
         send_far(0, 1).start()
 
-    for j in (2, 3, 1):
-        send_near(j).start()
-
     @pl.when(outer == 1)
     def _():
+        for j in (2, 3, 1):
+            send_near(j).start()
+
+    fill_own(spread_tail, half - head)
+    @pl.when(outer == 0)
+    def _():
+        for j in (2, 3, 1):
+            send_near(j).start()
+
+    @pl.when(outer == 1)
+    def _():
         send_far(1, 0).start()
 
+    gath[0, t] = own[0]
     share_core(0, t).start()
 
     fetches[2].wait()
@@ -485,7 +498,7 @@
         )
         return carry
 
-    lax.fori_loop(0, tokens // ROW_TILE, conv_rows, 0)
+    lax.fori_loop(0, tokens // ROW_TILE, conv_rows, 0, unroll=4)
     conv_core.start()
 
     def relay(k):
@@ -504,12 +517,12 @@
 
     @pl.when(outer == 1)
     def _():
-        for p in range(CONV_PARTS - 1):
+        for p in range(CONV_PARTS // 2):
             conv_y(t, p).start()
 
     normal_y.wait_recv()
     pair_peer = slots_of(y_peer)
-    spread_peer = spread_of(pair_peer, half)
+    spread_peer = spread_of(pair_peer, 0, half)
     for c in range(0, width, COLS):
         rows = jnp.dot(spread_peer, normal_peer[:, c : c + COLS], preferred_element_type=jnp.float32)
         rows = rows.astype(jnp.bfloat16).reshape(half, slots, COLS)
@@ -551,14 +564,14 @@
 
         @pl.when((k > 1) & (k <= half))
         def _():
+            result_peer[k] = (
+                part[k, y_peer].astype(jnp.float32) + from_core[1, k].astype(jnp.float32)
+            ).astype(jnp.bfloat16)
+            return_near_peer(k).start()
             result[k] = (
                 part[k, t].astype(jnp.float32) + from_core[0, k].astype(jnp.float32)
             ).astype(jnp.bfloat16)
             return_near(k).start()
-            result_peer[k] = (
-                part[k, y_peer].astype(jnp.float32) + from_core[1, k].astype(jnp.float32)
-            ).astype(jnp.bfloat16)
-            return_near_peer(k).start()
 
         @pl.when(k == 0)
         def _():
@@ -591,7 +604,7 @@
         @pl.when((i == 0) & (outer == 1))
         def _():
             relay(1)
-            conv_y(t, CONV_PARTS - 1).start()
+            conv_y(t, 2).start()
 
         @pl.when(i == outer)
         def _():
@@ -607,26 +620,26 @@
             relay(6)
             relay(7)
 
+        @pl.when((i == 7) & (outer == 1))
+        def _():
+            meet_y(5)
+
         meet_first = (i == n - 1) | ((outer == 0) & (i >= 4)) | ((outer == 1) & (lax.rem(i, 2) == 0) & (i < 6))
 
         @pl.when(meet_first)
         def _():
             meet_core(k)
 
-        @pl.when(i == 4)
+        @pl.when((i == 4) & (outer == 0))
         def _():
             meet_y(1)
+            relay(6)
 
         @pl.when((i == 5) & (outer == 0))
         def _():
-            relay(6)
             meet_y(5)
             relay(7)
 
-        @pl.when((i == 7) & (outer == 1))
-        def _():
-            meet_y(5)
-
         @pl.when(i + 1 < n)
         def _():
             share_y(later, y_peer).wait_recv()
@@ -636,9 +649,9 @@
         def _():
             meet_core(k)
 
-        @pl.when((i == 2) & (outer == 0))
-        def _():
-            conv_y(t, 2).start()
+        @pl.when((i == 3) & (outer == 1))
+        def _():
+            meet_y(1)
 
         return carry // n
 
@@ -646,13 +659,14 @@
 
     @pl.when(outer == 0)
     def _():
-        conv_y(t, CONV_PARTS - 1).start()
+        conv_y(t, 2).start()
+
+    conv_y(t, 3).start()
 
     meet_y(6)
 
     meet_y(7)
     for j in (1, 2, 3):
-        remote(result.at[j], returned.at[j], 7, j, (e, core_peer)).wait_recv()
         remote(result.at[j], returned_peer.at[j], 8, j, (e, core_peer)).wait_recv()
     weight_y.wait_recv()
     peer_share = share_of(pair_peer, weight_peer, 0, half)
@@ -678,6 +692,8 @@
 
     shared = gated(normal[...], sh_gate[...], sh_up[...])
     near_share = share_of(pair, weight_ref, 0, half)
+    for j in (1, 2, 3):
+        remote(result.at[j], returned.at[j], 7, j, (e, core_peer)).wait_recv()
     for c in range(0, width, COLS):
         rows = returned[0:half, :, c : c + COLS].reshape(half * slots, COLS)
         piece = jnp.dot(shared, sh_down[:, c : c + COLS], preferred_element_type=jnp.float32)

time: 91.8 us -> 88.7 us (0.966)
  Pallas kernels: 89.2 us -> 86.3 us
    pallas_call x1, Pallas kernels: 89.2 us -> 86.3 us  [fused(): pl.pallas_call(functools.partial(fused_kernel, n, slots, reach), out_shap...]
where the time goes in v3:
time: 88.7 us; the launch traced here: 88.5 us
  Pallas kernels  86.3 us (97%)
  local copies, waits for them, and re-layouts  1.59 us (2%)
    pallas_call x1, Pallas kernels, fused(): pl.pallas_call(functools.partial(fused_kernel, n, slots, reach), out_shap...  86.3 us

profile of v3, /device:TPU:0, one launch (start us, length us, event | category | flops | bytes accessed | tf_op | source)
XLA Modules:
  0.0 88.5 jit_solution(5171258493340535018)
XLA Ops:
  0.6 86.3 %shard_map.149 = (bf16[512,512]{1,0:T(8,128)(2,1)S(1)}, bf16[128,2048]{1,0:T(8,128)(2,1)S(1)}) custom-call(bf16[128,2048]{1,0:T(8,128)(2,1)} %conv_hbm.1, f32[31,2048]{1,0:T(8,128)} %taps_hbm.1, f32[1,2048]{1,0:T(1,128)} %bitcast.4, bf16[2048,512]{1,0:T(8,128)(2,1)} %out_w_hbm.1, bf16[128,2048]{1,0:T(8,128)(2,1)} %moe_hbm.1, f32[1,2048]{1,0:T(1,128)} %bitcast.5, ...), custom_call_target="tpu_custom_call" | custom-call | tf_op jit(solution)/shard_map/pallas_call | solution.py:779
  86.9 0.8 copy.18
  87.7 0.8 copy.19

commit v4 on v3

--- a/solution.py
+++ b/solution.py
@@ -612,8 +612,7 @@
 
         @pl.when((i == 0) & (outer == 0))
         def _():
-            for p in range(CONV_PARTS // 2):
-                conv_y(t, p).start()
+            conv_y(t, 0).start()
 
         @pl.when((i == 2) & (outer == 1))
         def _():
@@ -632,8 +631,8 @@
 
         @pl.when((i == 4) & (outer == 0))
         def _():
+            relay(6)
             meet_y(1)
-            relay(6)
 
         @pl.when((i == 5) & (outer == 0))
         def _():
@@ -659,6 +658,7 @@
 
     @pl.when(outer == 0)
     def _():
+        conv_y(t, 1).start()
         conv_y(t, 2).start()
 
     conv_y(t, 3).start()

time: 88.7 us -> 86.9 us (0.980)
  Pallas kernels: 86.3 us -> 84.5 us
    pallas_call x1, Pallas kernels: 86.3 us -> 84.5 us  [fused(): pl.pallas_call(functools.partial(fused_kernel, n, slots, reach), out_shap...]
where the time goes in v4:
time: 86.9 us; the launch traced here: 86.7 us
  Pallas kernels  84.5 us (97%)
  local copies, waits for them, and re-layouts  1.59 us (2%)
    pallas_call x1, Pallas kernels, fused(): pl.pallas_call(functools.partial(fused_kernel, n, slots, reach), out_shap...  84.5 us

profile of v4, /device:TPU:0, one launch (start us, length us, event | category | flops | bytes accessed | tf_op | source)
XLA Modules:
  0.0 86.7 jit_solution(7992077809638454036)
XLA Ops:
  0.6 84.5 %shard_map.149 = (bf16[512,512]{1,0:T(8,128)(2,1)S(1)}, bf16[128,2048]{1,0:T(8,128)(2,1)S(1)}) custom-call(bf16[128,2048]{1,0:T(8,128)(2,1)} %conv_hbm.1, f32[31,2048]{1,0:T(8,128)} %taps_hbm.1, f32[1,2048]{1,0:T(1,128)} %bitcast.4, bf16[2048,512]{1,0:T(8,128)(2,1)} %out_w_hbm.1, bf16[128,2048]{1,0:T(8,128)(2,1)} %moe_hbm.1, f32[1,2048]{1,0:T(1,128)} %bitcast.5, ...), custom_call_target="tpu_custom_call" | custom-call | tf_op jit(solution)/shard_map/pallas_call | solution.py:779
  85.1 0.8 copy.18
  85.9 0.8 copy.19
